TPU v7x, 32 devices: a whole 2x2x4 slice. The times are simulated.
32 devices in a mesh: grp: 2 (over y), fs: 4 (over z), tp: 4 (over x, core).
Axes of the slice: x: 2, y: 2, z: 4, core: 2. Of those that a mesh axis runs over, the one named last changes fastest.
Arguments:
- prompt: bfloat16 [1024, 2048], P(('grp', 'fs', 'tp')), parts along dimension 0, may hold values from -6 to 6
- norm_gain: float32 [2048], P('fs'), may hold values from 0.1 to 1.9
- up_weight: float32 [2048, 8192], P('fs', 'tp'), may hold values from -0.125 to 0.125
- down_weight: float32 [8192, 2048], P('fs', 'tp'), may hold values from -0.0625 to 0.0625
Outputs:
- up_serving: bfloat16 [4096, 8192], P('grp', 'fs'), parts along dimension 0
- down_serving: bfloat16 [8192, 4096], P('fs', 'grp'), parts along dimension 1
- mlp_output: bfloat16 [1024, 2048], P(('grp', 'fs', 'tp')), parts along dimension 0
There are 2 independent parts, one for each index of `grp`. A program takes and returns all parts, laid end to end along the dimension named above; an argument that names none is the same for every part. Nothing has to cross between parts.
All inputs are finite; a program needn't handle non-finite values.
Results may differ from a plain program's by a relative error of at most 0.024.
Values may be sent and summed in bfloat16 or wider, within the bound.
A program may use at most 128 MiB of HBM per device.

v0:
```python
import functools

import jax
import jax.numpy as jnp
from jax import lax
from jax.experimental import pallas as pl
from jax.experimental.pallas import tpu as pltpu
from jax.sharding import PartitionSpec as P

epsilon = 1e-06
CORES = 2
PIECES = 4
UP_STEPS = 4
DOWN_SPLIT = 0
LAG_A = 1
LAG_B = 3
MESH = pl.DeviceIdType.MESH


def kernel(
    groups, fs_count, tp_count, up_steps, down_chunks, down_split,
    ub, db, prompt, up_v, down_v, out_v,
    nb, nall, proj, hidden, pbuf, rbuf, stage,
    up_send, stage_recv, z_send, up_recv, upf_send, own_send, own_recv,
    dn_send, dn_recv, dnf_send, sib_send, sib_recv,
    n_send, n_recv, r_send, r_recv,
):
    y, z, t = lax.axis_index("grp"), lax.axis_index("fs"), lax.axis_index("tp")
    x, c = t // CORES, lax.rem(t, CORES)
    chips = tp_count // CORES
    ratio, rows, units = ub.shape
    chunk = rows // (up_steps * CORES * groups)
    width = db.shape[1]
    dchunk = units // down_chunks
    tokens = prompt.shape[0]
    sibling = (y, z, x * CORES + 1 - c)
    t_src = z // ratio
    x_src, c_src = t_src // CORES, lax.rem(t_src, CORES)
    same_x = x == x_src

    def remote(src, dst, ssem, rsem, dev):
        return pltpu.make_async_remote_copy(
            src_ref=src, dst_ref=dst, send_sem=ssem, recv_sem=rsem, device_id=dev, device_id_type=MESH
        )

    def n_copy(d):
        dst = nall.at[pl.ds(pl.multiple_of(z * tokens, tokens), tokens), :]
        return remote(nb, dst, n_send.at[d], n_recv.at[z], (y, lax.rem(z + d, fs_count), t))

    def up_at(zr, k):
        return up_v.at[pl.ds(pl.multiple_of(zr * rows + k * chunk, chunk), chunk), :]

    def up_index(m, core, owner):
        return (m * CORES + core) * groups + owner

    def src_at(j, m, cd):
        k = up_index(m, cd, y)
        return ub.at[j, pl.ds(pl.multiple_of(k * chunk, chunk), chunk), :]

    def up_x(j, m, cd, dx):
        dev = (y, z, lax.rem(x + dx, chips) * CORES + c)
        sem = up_send.at[j, m, cd, dx]
        return remote(src_at(j, m, cd), stage.at[x, j, m, cd], sem, stage_recv.at[x, j, m, cd], dev)

    def up_x_own(j, m, cd, dx):
        dev = (y, z, lax.rem(x + dx, chips) * CORES + cd)
        k = up_index(m, cd, y)
        return remote(src_at(j, m, cd), up_at(z, k), up_send.at[j, m, cd, dx], up_recv.at[z, k], dev)

    def up_x_all(act):
        for m in range(up_steps):
            for cd in range(CORES):
                for j in range(ratio):
                    mine = t * ratio + j == z
                    for dx in range(1, chips):
                        @pl.when(mine)
                        def _():
                            act(up_x_own(j, m, cd, dx))

                        @pl.when(jnp.logical_not(mine))
                        def _():
                            act(up_x(j, m, cd, dx))

    def up_z(j, m, cd, dx):
        xs = lax.rem(x + dx, chips)
        src = src_at(j, m, cd) if dx == 0 else stage.at[xs, j, m, cd]
        k = up_index(m, cd, y)
        dev = (y, (xs * CORES + c) * ratio + j, x * CORES + cd)
        return remote(src, up_at(z, k), z_send.at[j, m, cd, dx], up_recv.at[z, k], dev)

    def up_z_one(j, m, cd, dx, act):
        xs = lax.rem(x + dx, chips)

        @pl.when((xs * CORES + c) * ratio + j != z)
        def _():
            act(j, m, cd, dx)

    def go_z(j, m, cd, dx):
        if dx > 0:
            xs = lax.rem(x + dx, chips)
            at = stage.at[xs, j, m, cd]
            remote(at, at, up_send.at[j, m, cd, dx], stage_recv.at[xs, j, m, cd], sibling).wait_recv()
        up_z(j, m, cd, dx).start()

    own_j = lax.rem(z, ratio)
    own_rows = pl.ds(pl.multiple_of(z * rows, rows), rows)

    def own_copy():
        return remote(ub.at[own_j], up_v.at[own_rows, :], own_send, own_recv, sibling)

    def sib_copy():
        cols = pl.ds(pl.multiple_of(t * width, width), width)
        return remote(db, down_v.at[:, cols], sib_send, sib_recv, sibling)

    def dn_at(ts, k):
        return down_v.at[
            pl.ds(pl.multiple_of(k * dchunk, dchunk), dchunk), pl.ds(pl.multiple_of(ts * width, width), width)
        ]

    def dn_first(k, dx):
        src = db.at[pl.ds(pl.multiple_of(k * dchunk, dchunk), dchunk), :]
        dev = (y, z, lax.rem(x + dx, chips) * CORES + c)
        return remote(src, dn_at(t, k), dn_send.at[k, dx], dn_recv.at[t, k], dev)

    def dn_sends(act):
        for n in range(down_split):
            for dx in range(1, chips):
                act(dn_first(n * groups + y, dx))
        for k in range(down_split * groups, down_chunks):
            for dx in range(1, chips):
                act(dn_first(k, dx))

    start = lambda copy: copy.start()

    for m in range(1):
        for cd in range(CORES):
            for j in range(ratio):
                up_z_one(j, m, cd, 0, go_z)
    up_x_all(start)

    @pl.when(t == t_src)
    def _():
        own_copy().start()

    sib_copy().start()
    dn_sends(start)

    widened = prompt[...].astype(jnp.float32)
    scale = lax.rsqrt(jnp.mean(widened * widened, axis=-1, keepdims=True) + epsilon)
    nb[...] = (widened * scale).astype(jnp.bfloat16)

    def up_y(zr, k, g):
        dev = (lax.rem(y + g, groups), z, t)
        return remote(up_at(zr, k), up_at(zr, k), upf_send.at[zr, k, g], up_recv.at[zr, k], dev)

    def up_s(zr, k):
        return remote(up_at(zr, k), up_at(zr, k), upf_send.at[zr, k, 0], up_recv.at[zr, k], sibling)

    def dn_y(ts, k, g):
        dev = (lax.rem(y + g, groups), z, t)
        return remote(dn_at(ts, k), dn_at(ts, k), dnf_send.at[ts, k, g], dn_recv.at[ts, k], dev)

    def dn_s(ts, k):
        return remote(dn_at(ts, k), dn_at(ts, k), dnf_send.at[ts, k, 0], dn_recv.at[ts, k], sibling)

    def if_remote(d, fn):
        if d == 0:
            pl.when(jnp.logical_not(same_x))(fn)
        else:
            fn()

    def up_a(m, d):
        def go():
            zr, k = lax.rem(z + d, fs_count), up_index(m, c, y)
            up_s(zr, k).wait_recv()
            for g in range(1, groups):
                up_y(zr, k, g).start()
            up_s(zr, k).start()

        if_remote(d, go)

    def up_b(m, d):
        def go():
            zr = lax.rem(z + d, fs_count)
            for g in range(1, groups):
                k = up_index(m, c, lax.rem(y + g, groups))
                up_s(zr, k).wait_recv()
                up_s(zr, k).start()

        if_remote(d, go)

    def up_c(d):
        def go():
            zr = lax.rem(z + d, fs_count)
            for m in range(up_steps):
                for owner in range(groups):
                    up_s(zr, up_index(m, 1 - c, owner)).wait_recv()

        if_remote(d, go)

    def up_f(d):
        def go():
            zr = lax.rem(z + d, fs_count)
            for m in range(up_steps):
                for owner in range(groups):
                    up_s(zr, up_index(m, c, owner)).wait_send()
                for g in range(1, groups):
                    up_y(zr, up_index(m, c, y), g).wait_send()

        if_remote(d, go)

    def dn_src(dx):
        return lax.rem(x + dx, chips) * CORES + c

    def dn_a(n, dx):
        ts, k = dn_src(dx), n * groups + y
        dn_s(ts, k).wait_recv()
        for g in range(1, groups):
            dn_y(ts, k, g).start()
        dn_s(ts, k).start()

    def dn_b(n, dx):
        for g in range(1, groups):
            ts, k = dn_src(dx), n * groups + lax.rem(y + g, groups)
            dn_s(ts, k).wait_recv()
            dn_s(ts, k).start()

    def dn_n(k, dx):
        dn_s(dn_src(dx), k).wait_recv()
        dn_s(dn_src(dx), k).start()

    for m in range(up_steps + LAG_B):
        if m < up_steps:
            for cd in range(CORES):
                for j in range(ratio):
                    if m + 1 < up_steps:
                        up_z_one(j, m + 1, cd, 0, go_z)
                    for dx in range(1, chips):
                        up_z_one(j, m, cd, dx, go_z)
        if LAG_A <= m < up_steps + LAG_A:
            for d in range(fs_count):
                up_a(m - LAG_A, d)
        if m >= LAG_B:
            for d in range(fs_count):
                up_b(m - LAG_B, d)
    for n in range(down_split):
        for dx in range(1, chips):
            dn_a(n, dx)

    my_cols = pl.ds(pl.multiple_of(t * width, width), width)
    piece = units // down_chunks

    @pl.loop(0, down_chunks)
    def _(i):
        part = pl.ds(pl.multiple_of(i * piece, piece), piece)
        down_v[part, my_cols] = db[part, :]

    @pl.when(t == t_src)
    def _():
        @pl.loop(0, rows // chunk)
        def _(i):
            part = pl.ds(pl.multiple_of(i * chunk, chunk), chunk)
            up_v[pl.ds(pl.multiple_of(z * rows + i * chunk, chunk), chunk), :] = ub[own_j, part, :]

    nall[pl.ds(pl.multiple_of(z * tokens, tokens), tokens), :] = nb[...]

    @pl.loop(1, fs_count)
    def _(d):
        n_copy(d).start()

    for d in range(fs_count):
        up_c(d)

    @pl.when(jnp.logical_and(same_x, t != t_src))
    def _():
        own_copy().wait_recv()

    @pl.loop(1, fs_count)
    def _(d):
        zr = lax.rem(z + d, fs_count)
        dst = nall.at[pl.ds(pl.multiple_of(zr * tokens, tokens), tokens), :]
        remote(nb, dst, n_send.at[d], n_recv.at[zr], (y, zr, t)).wait_recv()

    depth = prompt.shape[1]
    kb = 256
    nb_tile = min(units, 1024)

    rest = [functools.partial(dn_b, n, dx) for n in range(down_split) for dx in range(1, chips)]
    rest += [
        functools.partial(dn_n, k, dx)
        for k in range(down_split * groups, down_chunks)
        for dx in range(1, chips)
    ]
    pieces = depth // kb
    done = 0
    for i in range(pieces):
        for j in range(units // nb_tile):
            col = pl.ds(j * nb_tile, nb_tile)
            term = jnp.dot(
                nall[:, i * kb : (i + 1) * kb],
                up_v[i * kb : (i + 1) * kb, col],
                preferred_element_type=jnp.float32,
            )
            if i == 0:
                proj[:, col] = term
            else:
                proj[:, col] += term
        upto = len(rest) * (i + 1) // pieces
        for fn in rest[done:upto]:
            fn()
        done = upto

    positive = jnp.maximum(proj[...], 0.0)
    hidden[...] = (positive * positive).astype(jnp.bfloat16)

    def out_copy(ts, d):
        zt = lax.rem(z + d, fs_count)
        cols = pl.ds(pl.multiple_of(ts * width, width), width)
        return remote(pbuf.at[zt, :, cols], rbuf.at[z, :, cols], r_send.at[ts, d], r_recv.at[z, ts], (y, zt, t))

    def block(ts):
        cols = pl.ds(pl.multiple_of(ts * width, width), width)
        part = jnp.dot(hidden[...], down_v[:, cols], preferred_element_type=jnp.float32).astype(jnp.bfloat16)
        pbuf[:, :, cols] = part.reshape(fs_count, tokens, width)

    def send_block(ts):
        @pl.loop(1, fs_count)
        def _(d):
            out_copy(ts, d).start()

    order = [t, x * CORES + 1 - c]
    for dx in range(1, chips):
        order += [dn_src(dx), lax.rem(x + dx, chips) * CORES + 1 - c]
    for i, ts in enumerate(order):
        if i == 1:
            sib_copy().wait_recv()
        if i >= CORES and i % CORES == 1:
            for k in range(down_chunks):
                dn_s(ts, k).wait_recv()
        block(ts)
        if i > 0:
            send_block(order[i - 1])
    send_block(order[-1])

    for d in range(fs_count):
        up_f(d)
    for dx in range(1, chips):
        ts = dn_src(dx)
        for k in range(down_chunks):
            dn_s(ts, k).wait_send()
        for n in range(down_split):
            for g in range(1, groups):
                dn_y(ts, n * groups + y, g).wait_send()
    up_x_all(lambda copy: copy.wait_send())
    for m in range(up_steps):
        for cd in range(CORES):
            for j in range(ratio):
                for dx in range(chips):
                    up_z_one(j, m, cd, dx, lambda *at: up_z(*at).wait_send())
    dn_sends(lambda copy: copy.wait_send())
    sib_copy().wait_send()

    @pl.when(t == t_src)
    def _():
        own_copy().wait_send()

    @pl.loop(1, fs_count)
    def _(d):
        n_copy(d).wait_send()

    total = pbuf[z].astype(jnp.float32)

    @pl.loop(1, fs_count)
    def _(d):
        zr = lax.rem(z + d, fs_count)
        for ts in range(tp_count):
            cols = pl.ds(ts * width, width)
            remote(pbuf.at[zr, :, cols], rbuf.at[zr, :, cols], r_send.at[ts, d], r_recv.at[zr, ts], (y, zr, t)).wait()

    for d in range(1, fs_count):
        total += rbuf[lax.rem(z + d, fs_count)].astype(jnp.float32)
    out_v[...] = total.astype(jnp.bfloat16)


def write_out(up_v, down_v, out_v, up_out, down_out, mlp_out, sems):
    copies = [pltpu.make_async_copy(out_v, mlp_out, sems.at[2 * PIECES])]
    for n, (src, dst) in enumerate(((up_v, up_out), (down_v, down_out))):
        step = src.shape[0] // PIECES
        for i in range(PIECES):
            part = pl.ds(i * step, step)
            copies.append(pltpu.make_async_copy(src.at[part, :], dst.at[part, :], sems.at[n * PIECES + i]))
    for copy in copies:
        copy.start()
    for copy in copies:
        copy.wait()


def per_device(groups, prompt, norm_gain, up_weight, down_weight):
    tp_count, fs_count = lax.axis_size("tp"), lax.axis_size("fs")
    rows, wide = up_weight.shape
    units, width = down_weight.shape
    tokens, depth = prompt.shape
    ratio = wide // units
    folded = (norm_gain[:, None] * up_weight).astype(jnp.bfloat16)
    folded = folded.reshape(rows, ratio, units).transpose(1, 0, 2)
    down_local = down_weight.astype(jnp.bfloat16)
    up_steps = max(1, min(UP_STEPS, rows // (CORES * groups * 16)))
    down_chunks = 8
    down_split = DOWN_SPLIT
    chips = tp_count // CORES
    kc = up_steps * CORES * groups
    dma = pltpu.SemaphoreType.DMA
    vmem = pl.BlockSpec(memory_space=pltpu.VMEM)
    up_v, down_v, out_v = pl.pallas_call(
        functools.partial(kernel, groups, fs_count, tp_count, up_steps, down_chunks, down_split),
        out_shape=(
            pltpu.VMEM((depth, units), jnp.bfloat16),
            pltpu.VMEM((units, depth), jnp.bfloat16),
            jax.ShapeDtypeStruct((tokens, depth), jnp.bfloat16),
        ),
        in_specs=[vmem] * 3,
        out_specs=(vmem,) * 3,
        scratch_shapes=[
            pltpu.VMEM((tokens, depth), jnp.bfloat16),
            pltpu.VMEM((fs_count * tokens, depth), jnp.bfloat16),
            pltpu.VMEM((fs_count * tokens, units), jnp.float32),
            pltpu.VMEM((fs_count * tokens, units), jnp.bfloat16),
            pltpu.VMEM((fs_count, tokens, depth), jnp.bfloat16),
            pltpu.VMEM((fs_count, tokens, depth), jnp.bfloat16),
            pltpu.VMEM((chips, ratio, up_steps, CORES, rows // kc, units), jnp.bfloat16),
            dma((ratio, up_steps, CORES, chips)),
            dma((chips, ratio, up_steps, CORES)),
            dma((ratio, up_steps, CORES, chips)),
            dma((fs_count, kc)),
            dma((fs_count, kc, groups)),
            dma, dma,
            dma((down_chunks, chips)),
            dma((tp_count, down_chunks)),
            dma((tp_count, down_chunks, groups)),
            dma, dma,
            dma((fs_count,)),
            dma((fs_count,)),
            dma((tp_count, fs_count)),
            dma((fs_count, tp_count)),
        ],
        compiler_params=pltpu.CompilerParams(has_side_effects=True, vmem_limit_bytes=24 * 1024 * 1024),
    )(folded, down_local, prompt)
    any_space = pl.BlockSpec(memory_space=pl.ANY)
    return pl.pallas_call(
        write_out,
        out_shape=(
            jax.ShapeDtypeStruct(up_v.shape, jnp.bfloat16),
            jax.ShapeDtypeStruct(down_v.shape, jnp.bfloat16),
            jax.ShapeDtypeStruct(out_v.shape, jnp.bfloat16),
        ),
        in_specs=[vmem] * 3,
        out_specs=(any_space,) * 3,
        scratch_shapes=[dma((2 * PIECES + 1,))],
        compiler_params=pltpu.CompilerParams(vmem_limit_bytes=1024 * 1024),
        cost_estimate=pl.CostEstimate(flops=0, bytes_accessed=4 * depth * units * 2, transcendentals=0),
    )(up_v, down_v, out_v)


def solution(mesh):
    return jax.shard_map(
        functools.partial(per_device, mesh.shape["grp"]),
        mesh=mesh,
        in_specs=(P(("grp", "fs", "tp"), None), P("fs"), P("fs", "tp"), P("fs", "tp")),
        out_specs=(P("grp", "fs"), P("fs", "grp"), P(("grp", "fs", "tp"), None)),
        check_vma=False,
    )
```

profile of v0, /device:TPU:0, one launch (start us, length us, event | category | flops | bytes accessed | tf_op | source)
XLA Modules:
  0.0 107.4 jit_solution(15901315902133850073)
XLA Ops:
  0.6 0.0 copy-start.1
  0.6 2.6 %fusion.ub = bf16[1,512,2048]{2,1,0:T(8,128)(2,1)S(1)} fusion(f32[512,2048]{1,0:T(8,128)} %param.6, f32[512]{0:T(512)} %param.5), kind=kLoop, calls=%fused_computation.1 | loop fusion | flops 2097152 | bytes 6293504 | tf_op jit(solution)/shard_map/transpose;reshape | solution.py:405
  3.3 0.8 copy-done.1
  4.1 0.0 copy-start
  4.1 0.3 convert_element_type.7.db
  4.4 0.6 copy-done
  5.0 96.4 %shard_map.67 = (bf16[2048,2048]{1,0:T(8,128)(2,1)S(1)}, bf16[2048,2048]{1,0:T(8,128)(2,1)S(1)}, bf16[32,2048]{1,0:T(8,128)(2,1)S(1)}) custom-call(bf16[1,512,2048]{2,1,0:T(8,128)(2,1)S(1)} %fusion.ub, bf16[2048,512]{1,0:T(8,128)(2,1)S(1)} %convert_element_type.7.db, bf16[32,2048]{1,0:T(8,128)(2,1)S(1)} %copy-done), custom_call_target="tpu_custom_call" | custom-call | tf_op jit(solution)/shard_map/pallas_call | solution.py:414
  101.4 6.0 %shard_map.68 = (bf16[2048,2048]{1,0:T(8,128)(2,1)}, bf16[2048,2048]{1,0:T(8,128)(2,1)}, bf16[32,2048]{1,0:T(8,128)(2,1)}) custom-call(bf16[2048,2048]{1,0:T(8,128)(2,1)S(1)} %get-tuple-element.6.up_v, bf16[2048,2048]{1,0:T(8,128)(2,1)S(1)} %get-tuple-element.7.down_v, bf16[32,2048]{1,0:T(8,128)(2,1)S(1)} %get-tuple-element.8.out_v), custom_call_target="tpu_custom_call" | custom-call | bytes 33554432 | tf_op jit(solution)/shard_map/pallas_call | solution.py:449
Async XLA Ops:
  0.6 3.5 %copy-start.1 = (f32[2048,512]{1,0:T(8,128)S(1)}, f32[2048,512]{1,0:T(8,128)}, u32[]{:S(2)}) copy-start(f32[2048,512]{1,0:T(8,128)} %param.7) | copy-start | bytes 12582916
  4.1 0.9 copy-start
where the time goes:
time: 108 us; the launch traced here: 107 us
  Pallas kernels  102 us (94%)
  other arithmetic  2.89 us (3%)
  local copies, waits for them, and re-layouts  1.46 us (1%)
    pallas_call x1, Pallas kernels, per_device(): pl.pallas_call(functools.partial(kernel, groups, fs_count, tp_count, up_s...  96.4 us
    pallas_call x1, Pallas kernels, per_device(): pl.pallas_call(write_out, out_shape=(jax.ShapeDtypeStruct(up_v.shape, jnp...  5.98 us
    another operation x1, other arithmetic, per_device(): folded = folded.reshape(rows, ratio, units).transpose(1, 0, 2)  2.62 us

commit v1 on v0

v1 whole, which is shorter than its diff:
```python
import functools

import jax
import jax.numpy as jnp
from jax import lax
from jax.experimental import pallas as pl
from jax.experimental.pallas import tpu as pltpu
from jax.sharding import PartitionSpec as P

epsilon = 1e-06
CORES = 2
PIECES = 4
UP_STEPS = 8
READS = 4
LANES = 128
K_PIECES = 4
WHOLE_PART = 0.5
AHEAD = 2
STAGE = (0.05, 0.45)
ARRIVAL = ((0.06, 0.52), (0.13, 0.55), (0.18, 0.78), (0.22, 1.02))
LAG_Y = 0.2
ROWS = (0.12, 0.6)
MESH = pl.DeviceIdType.MESH


def rank(origin, at, count):
    half = count // 2
    far = (origin < half) != (at < half)
    inner = abs(2 * origin - count + 1)
    if abs(2 * at - count + 1) > 1:
        return (far, -inner)
    return (-inner, not far)


def kernel(
    groups, fs_count, tp_count, up_steps, whole_cols, k_pieces,
    gain, up_w, down_w, prompt, up_v, down_v, out_v,
    gain_v, prompt_v, up_f, down_f, gain_col,
    ub, nb, nall, proj, hidden, pbuf, rbuf, stage,
    in_sem, up_send, stage_recv, z_send, up_recv, upf_send, own_send, own_recv,
    dn_send, dn_recv, dnf_send, sib_send, sib_recv,
    n_send, n_recv, r_send, r_recv,
):
    y, z, t = lax.axis_index("grp"), lax.axis_index("fs"), lax.axis_index("tp")
    x, c = t // CORES, lax.rem(t, CORES)
    chips = tp_count // CORES
    ratio, rows, units = ub.shape
    chunk = rows // (up_steps * CORES * groups)
    width = down_w.shape[1]
    col_chunks = width // LANES
    k_rows = units // k_pieces
    tokens = prompt.shape[0]
    sibling = (y, z, x * CORES + 1 - c)
    t_src = z // ratio
    x_src, c_src = t_src // CORES, lax.rem(t_src, CORES)
    same_x = x == x_src

    up_part = rows // READS
    down_part = units // READS

    def up_read(i):
        at = pl.ds(i * up_part, up_part)
        return pltpu.make_async_copy(up_w.at[at, :], up_f.at[at, :], in_sem.at[2 + i])

    def down_read(i):
        at = pl.ds(i * down_part, down_part)
        return pltpu.make_async_copy(down_w.at[at, :], down_f.at[at, :], in_sem.at[2 + READS + i])

    gain_read = pltpu.make_async_copy(gain, gain_v, in_sem.at[0])
    prompt_read = pltpu.make_async_copy(prompt, prompt_v, in_sem.at[1])
    gain_read.start()
    prompt_read.start()
    for i in range(READS):
        up_read(i).start()
    for i in range(READS):
        down_read(i).start()

    barrier = pltpu.get_barrier_semaphore()
    peers = [sibling]
    peers += [(y, lax.rem(z + d, fs_count), x * CORES + cc) for d in range(1, fs_count) for cc in range(CORES)]
    peers += [(y, z, lax.rem(x + d, chips) * CORES + cc) for d in range(1, chips) for cc in range(CORES)]
    peers += [(lax.rem(y + g, groups), z, t) for g in range(1, groups)]
    for peer in peers:
        pl.semaphore_signal(barrier, inc=1, device_id=peer, device_id_type=MESH)

    gain_read.wait()
    gain_col[...] = jnp.broadcast_to(gain_v[...], (LANES, rows)).T
    prompt_read.wait()
    widened = prompt_v[...].astype(jnp.float32)
    scale = lax.rsqrt(jnp.mean(widened * widened, axis=-1, keepdims=True) + epsilon)
    nb[...] = (widened * scale).astype(jnp.bfloat16)
    step = min(16, up_part)
    for n in range(READS):
        up_read(n).wait()

        @pl.loop(0, up_part // step)
        def _(i):
            at = pl.ds(pl.multiple_of(n * up_part + i * step, step), step)
            factor = gain_col[at, :]
            for j in range(ratio):
                for b in range(units // LANES):
                    piece = up_f[at, j * units + b * LANES : j * units + (b + 1) * LANES]
                    ub[j, at, b * LANES : (b + 1) * LANES] = (factor * piece).astype(jnp.bfloat16)

    pl.semaphore_wait(barrier, len(peers))

    def remote(src, dst, ssem, rsem, dev):
        return pltpu.make_async_remote_copy(
            src_ref=src, dst_ref=dst, send_sem=ssem, recv_sem=rsem, device_id=dev, device_id_type=MESH
        )

    def n_at(zr):
        return nall.at[pl.ds(pl.multiple_of(zr * tokens, tokens), tokens), :]

    def n_copy(zr, up, first):
        src = nb if first else n_at(zr)
        dev = (y, z + 1 if up else z - 1, t)
        return remote(src, n_at(zr), n_send.at[zr, int(up)], n_recv.at[zr], dev)

    def n_hop(h, act, wait):
        for up in (True, False):
            origin = z - h if up else z + h

            @pl.when(jnp.logical_and(origin >= 0, origin < fs_count))
            def _():
                if wait and h > 0:
                    remote(nb, n_at(origin), n_send.at[origin, int(up)], n_recv.at[origin], sibling).wait_recv()

                @pl.when(z < fs_count - 1 if up else z > 0)
                def _():
                    act(n_copy(origin, up, h == 0))

    def up_at(zr, k):
        return up_v.at[pl.ds(pl.multiple_of(zr * rows + k * chunk, chunk), chunk), :]

    def up_index(m, core, owner):
        return (m * CORES + core) * groups + owner

    def src_at(j, m, cd):
        k = up_index(m, cd, y)
        return ub.at[j, pl.ds(pl.multiple_of(k * chunk, chunk), chunk), :]

    def up_x(j, m, cd, dx):
        dev = (y, z, lax.rem(x + dx, chips) * CORES + c)
        sem = up_send.at[j, m, cd, dx]
        return remote(src_at(j, m, cd), stage.at[x, j, m, cd], sem, stage_recv.at[x, j, m, cd], dev)

    def up_x_own(j, m, cd, dx):
        dev = (y, z, lax.rem(x + dx, chips) * CORES + cd)
        k = up_index(m, cd, y)
        return remote(src_at(j, m, cd), up_at(z, k), up_send.at[j, m, cd, dx], up_recv.at[z, k], dev)

    def up_x_all(act):
        for m in range(up_steps):
            for cd in range(CORES):
                for j in range(ratio):
                    mine = t * ratio + j == z
                    for dx in range(1, chips):
                        @pl.when(mine)
                        def _():
                            act(up_x_own(j, m, cd, dx))

                        @pl.when(jnp.logical_not(mine))
                        def _():
                            act(up_x(j, m, cd, dx))

    def up_z(j, m, cd, dx):
        xs = lax.rem(x + dx, chips)
        src = src_at(j, m, cd) if dx == 0 else stage.at[xs, j, m, cd]
        k = up_index(m, cd, y)
        dev = (y, (xs * CORES + c) * ratio + j, x * CORES + cd)
        return remote(src, up_at(z, k), z_send.at[j, m, cd, dx], up_recv.at[z, k], dev)

    def up_z_one(j, m, cd, dx, act):
        xs = lax.rem(x + dx, chips)

        @pl.when((xs * CORES + c) * ratio + j != z)
        def _():
            act(j, m, cd, dx)

    def go_z(j, m, cd, dx):
        if dx > 0:
            xs = lax.rem(x + dx, chips)
            at = stage.at[xs, j, m, cd]
            remote(at, at, up_send.at[j, m, cd, dx], stage_recv.at[xs, j, m, cd], sibling).wait_recv()
        up_z(j, m, cd, dx).start()

    def z_own(m):
        for cd in range(CORES):
            for j in range(ratio):
                up_z_one(j, m, cd, 0, go_z)

    def z_staged(m):
        for cd in range(CORES):
            for j in range(ratio):
                for dx in range(1, chips):
                    up_z_one(j, m, cd, dx, go_z)

    own_j = lax.rem(z, ratio)
    own_rows = pl.ds(pl.multiple_of(z * rows, rows), rows)
    my_cols = pl.ds(pl.multiple_of(t * width, width), width)

    def own_copy():
        return remote(ub.at[own_j], up_v.at[own_rows, :], own_send, own_recv, sibling)

    def sib_copy():
        return remote(down_v.at[:, my_cols], down_v.at[:, my_cols], sib_send, sib_recv, sibling)

    def cols_of(ts, i):
        return pl.ds(pl.multiple_of(ts * width + i * LANES, LANES), LANES)

    def dn_at(ts, i, k):
        return down_v.at[pl.ds(pl.multiple_of(k * k_rows, k_rows), k_rows), cols_of(ts, i)]

    def dn_first(i, k, dx):
        dev = (y, z, lax.rem(x + dx, chips) * CORES + c)
        return remote(dn_at(t, i, k), dn_at(t, i, k), dn_send.at[i, k, dx], dn_recv.at[t, i, k], dev)

    def dn_sends(act):
        for i in range(col_chunks):
            if i < whole_cols:
                for k in range(k_pieces):
                    for dx in range(1, chips):
                        act(dn_first(i, k, dx))
            else:
                for n in range(k_pieces // groups):
                    for dx in range(1, chips):
                        act(dn_first(i, n * groups + y, dx))

    start = lambda copy: copy.start()
    n_hop(0, start, False)
    for m in range(min(AHEAD, up_steps)):
        z_own(m)
    up_x_all(start)

    @pl.when(t == t_src)
    def _():
        own_copy().start()

    down_step = min(64, down_part)
    for n in range(READS):
        down_read(n).wait()

        @pl.loop(0, down_part // down_step)
        def _(i):
            at = pl.ds(pl.multiple_of(n * down_part + i * down_step, down_step), down_step)
            down_v[at, my_cols] = down_f[at, :].astype(jnp.bfloat16)

    dn_sends(start)
    sib_copy().start()

    n_at(z)[...] = nb[...]

    @pl.when(t == t_src)
    def _():
        @pl.loop(0, rows // chunk)
        def _(i):
            part = pl.ds(pl.multiple_of(i * chunk, chunk), chunk)
            up_v[pl.ds(pl.multiple_of(z * rows + i * chunk, chunk), chunk), :] = ub[own_j, part, :]

    def up_y(zr, k, g):
        dev = (lax.rem(y + g, groups), z, t)
        return remote(up_at(zr, k), up_at(zr, k), upf_send.at[zr, k, g], up_recv.at[zr, k], dev)

    def up_s(zr, k):
        return remote(up_at(zr, k), up_at(zr, k), upf_send.at[zr, k, 0], up_recv.at[zr, k], sibling)

    def dn_y(ts, i, k, g):
        dev = (lax.rem(y + g, groups), z, t)
        return remote(dn_at(ts, i, k), dn_at(ts, i, k), dnf_send.at[ts, i, k, g], dn_recv.at[ts, i, k], dev)

    def dn_s(ts, i, k):
        return remote(dn_at(ts, i, k), dn_at(ts, i, k), dnf_send.at[ts, i, k, 0], dn_recv.at[ts, i, k], sibling)

    def if_remote(d, fn):
        if d == 0:
            pl.when(jnp.logical_not(same_x))(fn)
        else:
            fn()

    def source(d):
        if d == 0 or fs_count > 8:
            return lax.rem(z + d, fs_count)
        found = 0
        for at in range(fs_count):
            order = sorted((o for o in range(fs_count) if o != at), key=lambda o: rank(o, at, fs_count))
            found = jnp.where(z == at, order[d - 1], found)
        return found

    def up_a(m, d):
        def go():
            zr, k = source(d), up_index(m, c, y)
            up_s(zr, k).wait_recv()
            for g in range(1, groups):
                up_y(zr, k, g).start()
            up_s(zr, k).start()

        if_remote(d, go)

    def up_b(m, d):
        def go():
            zr = source(d)
            for g in range(1, groups):
                k = up_index(m, c, lax.rem(y + g, groups))
                up_s(zr, k).wait_recv()
                up_s(zr, k).start()

        if_remote(d, go)

    def up_c(d):
        def go():
            zr = source(d)
            for m in range(up_steps):
                for owner in range(groups):
                    up_s(zr, up_index(m, 1 - c, owner)).wait_recv()

        if_remote(d, go)

    def up_f(d):
        def go():
            zr = source(d)
            for m in range(up_steps):
                for owner in range(groups):
                    up_s(zr, up_index(m, c, owner)).wait_send()
                for g in range(1, groups):
                    up_y(zr, up_index(m, c, y), g).wait_send()

        if_remote(d, go)

    def dn_src(dx):
        return lax.rem(x + dx, chips) * CORES + c

    def dn_one(i, k, dx):
        ts = dn_src(dx)
        dn_s(ts, i, k).wait_recv()
        dn_s(ts, i, k).start()

    def dn_a(i, n, dx):
        ts, k = dn_src(dx), n * groups + y
        dn_s(ts, i, k).wait_recv()
        for g in range(1, groups):
            dn_y(ts, i, k, g).start()
        dn_s(ts, i, k).start()

    def dn_b(i, n, dx):
        for g in range(1, groups):
            dn_one(i, n * groups + lax.rem(y + g, groups), dx)

    part = functools.partial
    events = []
    for m in range(up_steps):
        share = m / max(1, up_steps - 1)
        when = STAGE[0] + (STAGE[1] - STAGE[0]) * share
        events.append((when, part(z_staged, m)))
        if m + AHEAD < up_steps:
            events.append((when + 0.001, part(z_own, m + AHEAD)))
        for d in range(fs_count):
            base, span = ARRIVAL[min(d, len(ARRIVAL) - 1)]
            when = max(base + (span - base) * share, STAGE[0] + (STAGE[1] - STAGE[0]) * share + 0.01) + 0.002 * d
            events.append((when, part(up_a, m, d)))
            events.append((when + LAG_Y, part(up_b, m, d)))
    for h in range(1, fs_count):
        when = ROWS[h - 1] if h <= len(ROWS) else 1.2 + h
        events.append((when, part(n_hop, h, start, True)))
    for i in range(whole_cols):
        for dx in range(1, chips):
            for k in range(k_pieces):
                events.append((1.1, part(dn_one, i, k, dx)))
    for _, event in sorted(events, key=lambda e: e[0]):
        event()

    for d in range(fs_count):
        up_c(d)

    @pl.when(jnp.logical_and(same_x, t != t_src))
    def _():
        own_copy().wait_recv()

    depth = prompt.shape[1]
    kb = 256
    nb_tile = min(units, 1024)

    split = range(whole_cols, col_chunks)
    rest = [part(dn_a, i, n, dx) for i in split for n in range(k_pieces // groups) for dx in range(1, chips)]
    pieces = depth // kb
    done = 0
    for i in range(pieces):
        for j in range(units // nb_tile):
            col = pl.ds(j * nb_tile, nb_tile)
            term = jnp.dot(
                nall[:, i * kb : (i + 1) * kb],
                up_v[i * kb : (i + 1) * kb, col],
                preferred_element_type=jnp.float32,
            )
            if i == 0:
                proj[:, col] = term
            else:
                proj[:, col] += term
        upto = len(rest) * (i + 1) // (2 * pieces)
        for fn in rest[done:upto]:
            fn()
        done = upto

    positive = jnp.maximum(proj[...], 0.0)
    hidden[...] = (positive * positive).astype(jnp.bfloat16)

    def r_copy(ts, i, wide, d):
        zt = lax.rem(z + d, fs_count)
        cols = pl.ds(pl.multiple_of(ts * width + i * LANES, LANES), wide)
        sems = r_send.at[ts, i, d], r_recv.at[z, ts, i]
        return remote(pbuf.at[zt, :, cols], rbuf.at[z, :, cols], *sems, (y, zt, t))

    def r_done(ts, i, wide, d):
        zr = lax.rem(z + d, fs_count)
        cols = pl.ds(pl.multiple_of(ts * width + i * LANES, LANES), wide)
        sems = r_send.at[ts, i, d], r_recv.at[zr, ts, i]
        remote(pbuf.at[zr, :, cols], rbuf.at[zr, :, cols], *sems, (y, zr, t)).wait()

    def block(ts, i, wide):
        cols = pl.ds(pl.multiple_of(ts * width + i * LANES, LANES), wide)
        part = jnp.dot(hidden[...], down_v[:, cols], preferred_element_type=jnp.float32).astype(jnp.bfloat16)
        pbuf[:, :, cols] = part.reshape(fs_count, tokens, wide)

    blocks = [(t, 0, width), (x * CORES + 1 - c, 0, width)]
    for i in range(col_chunks):
        for dx in range(1, chips):
            blocks += [(dn_src(dx), i, LANES), (lax.rem(x + dx, chips) * CORES + 1 - c, i, LANES)]

    def send_block(ts, i, wide):
        for d in range(1, fs_count):
            r_copy(ts, i, wide, d).start()

    last = None
    for index, (ts, i, wide) in enumerate(blocks):
        if index == 1:
            sib_copy().wait_recv()
        if index >= CORES:
            dx = 1 + (index - CORES) // CORES % (chips - 1)
            if (index - CORES) % CORES == 0 and i >= whole_cols:
                for n in range(k_pieces // groups):
                    dn_b(i, n, dx)
            if (index - CORES) % CORES == 1:
                for k in range(k_pieces):
                    dn_s(ts, i, k).wait_recv()
        block(ts, i, wide)
        if index < CORES:
            upto = len(rest) if index == CORES - 1 else (done + len(rest)) // 2
            for fn in rest[done:upto]:
                fn()
            done = upto
        if last is not None:
            send_block(*last)
        last = (ts, i, wide)
    send_block(*last)

    for d in range(fs_count):
        up_f(d)
    for dx in range(1, chips):
        ts = dn_src(dx)
        for i in range(col_chunks):
            for k in range(k_pieces):
                dn_s(ts, i, k).wait_send()
            if i >= whole_cols:
                for n in range(k_pieces // groups):
                    for g in range(1, groups):
                        dn_y(ts, i, n * groups + y, g).wait_send()
    up_x_all(lambda copy: copy.wait_send())
    for m in range(up_steps):
        for cd in range(CORES):
            for j in range(ratio):
                for dx in range(chips):
                    up_z_one(j, m, cd, dx, lambda *at: up_z(*at).wait_send())
    dn_sends(lambda copy: copy.wait_send())
    sib_copy().wait_send()

    @pl.when(t == t_src)
    def _():
        own_copy().wait_send()

    for h in range(fs_count):
        n_hop(h, lambda copy: copy.wait_send(), False)

    total = pbuf[z].astype(jnp.float32)
    for ts, i, wide in blocks:
        @pl.loop(1, fs_count)
        def _(d):
            r_done(ts, i, wide, d)

    for d in range(1, fs_count):
        total += rbuf[lax.rem(z + d, fs_count)].astype(jnp.float32)
    out_v[...] = total.astype(jnp.bfloat16)


def write_out(up_v, down_v, out_v, up_out, down_out, mlp_out, sems):
    copies = [pltpu.make_async_copy(out_v, mlp_out, sems.at[2 * PIECES])]
    for n, (src, dst) in enumerate(((up_v, up_out), (down_v, down_out))):
        step = src.shape[0] // PIECES
        for i in range(PIECES):
            part = pl.ds(i * step, step)
            copies.append(pltpu.make_async_copy(src.at[part, :], dst.at[part, :], sems.at[n * PIECES + i]))
    for copy in copies:
        copy.start()
    for copy in copies:
        copy.wait()


def per_device(groups, prompt, norm_gain, up_weight, down_weight):
    tp_count, fs_count = lax.axis_size("tp"), lax.axis_size("fs")
    rows, wide = up_weight.shape
    units, width = down_weight.shape
    tokens, depth = prompt.shape
    ratio = wide // units
    up_steps = max(1, min(UP_STEPS, rows // (CORES * groups * 16)))
    col_chunks = width // LANES
    whole_cols = int(col_chunks * WHOLE_PART)
    chips = tp_count // CORES
    kc = up_steps * CORES * groups
    k_pieces = K_PIECES
    f32, bf16 = jnp.float32, jnp.bfloat16
    dma = pltpu.SemaphoreType.DMA
    vmem = pl.BlockSpec(memory_space=pltpu.VMEM)
    hbm = pl.BlockSpec(memory_space=pltpu.HBM)
    up_v, down_v, out_v = pl.pallas_call(
        functools.partial(kernel, groups, fs_count, tp_count, up_steps, whole_cols, k_pieces),
        out_shape=(
            pltpu.VMEM((depth, units), bf16),
            pltpu.VMEM((units, depth), bf16),
            jax.ShapeDtypeStruct((tokens, depth), bf16),
        ),
        in_specs=[hbm] * 4,
        out_specs=(vmem,) * 3,
        scratch_shapes=[
            pltpu.VMEM((1, rows), f32),
            pltpu.VMEM((tokens, depth), bf16),
            pltpu.VMEM((rows, wide), f32),
            pltpu.VMEM((units, width), f32),
            pltpu.VMEM((rows, LANES), f32),
            pltpu.VMEM((ratio, rows, units), bf16),
            pltpu.VMEM((tokens, depth), bf16),
            pltpu.VMEM((fs_count * tokens, depth), bf16),
            pltpu.VMEM((fs_count * tokens, units), f32),
            pltpu.VMEM((fs_count * tokens, units), bf16),
            pltpu.VMEM((fs_count, tokens, depth), bf16),
            pltpu.VMEM((fs_count, tokens, depth), bf16),
            pltpu.VMEM((chips, ratio, up_steps, CORES, rows // kc, units), bf16),
            dma((2 + 2 * READS,)),
            dma((ratio, up_steps, CORES, chips)),
            dma((chips, ratio, up_steps, CORES)),
            dma((ratio, up_steps, CORES, chips)),
            dma((fs_count, kc)),
            dma((fs_count, kc, groups)),
            dma, dma,
            dma((col_chunks, k_pieces, chips)),
            dma((tp_count, col_chunks, k_pieces)),
            dma((tp_count, col_chunks, k_pieces, groups)),
            dma, dma,
            dma((fs_count, 2)),
            dma((fs_count,)),
            dma((tp_count, col_chunks, fs_count)),
            dma((fs_count, tp_count, col_chunks)),
        ],
        compiler_params=pltpu.CompilerParams(
            collective_id=0, has_side_effects=True, vmem_limit_bytes=40 * 1024 * 1024
        ),
    )(norm_gain.reshape(1, rows), up_weight, down_weight, prompt)
    any_space = pl.BlockSpec(memory_space=pl.ANY)
    return pl.pallas_call(
        write_out,
        out_shape=(
            jax.ShapeDtypeStruct(up_v.shape, bf16),
            jax.ShapeDtypeStruct(down_v.shape, bf16),
            jax.ShapeDtypeStruct(out_v.shape, bf16),
        ),
        in_specs=[vmem] * 3,
        out_specs=(any_space,) * 3,
        scratch_shapes=[dma((2 * PIECES + 1,))],
        compiler_params=pltpu.CompilerParams(vmem_limit_bytes=1024 * 1024),
        cost_estimate=pl.CostEstimate(flops=0, bytes_accessed=4 * depth * units * 2, transcendentals=0),
    )(up_v, down_v, out_v)


def solution(mesh):
    return jax.shard_map(
        functools.partial(per_device, mesh.shape["grp"]),
        mesh=mesh,
        in_specs=(P(("grp", "fs", "tp"), None), P("fs"), P("fs", "tp"), P("fs", "tp")),
        out_specs=(P("grp", "fs"), P("fs", "grp"), P(("grp", "fs", "tp"), None)),
        check_vma=False,
    )
```

time: 108 us -> 97 us (0.90)
  Pallas kernels: 102 us -> 95.3 us
  other arithmetic: 2.89 us -> 0 us
    pallas_call x1, Pallas kernels: 96.4 us -> 89.3 us  [per_device(): pl.pallas_call(functools.partial(kernel, groups, fs_count, tp_count, up_s...]
    another operation x1 -> x0, other arithmetic: 2.62 us -> none  [per_device(): folded = folded.reshape(rows, ratio, units).transpose(1, 0, 2)]
where the time goes in v1:
time: 97 us; the launch traced here: 96.8 us
  Pallas kernels  95.3 us (98%)
    pallas_call x1, Pallas kernels, per_device(): pl.pallas_call(functools.partial(kernel, groups, fs_count, tp_count, up_s...  89.3 us
    pallas_call x1, Pallas kernels, per_device(): pl.pallas_call(write_out, out_shape=(jax.ShapeDtypeStruct(up_v.shape, bf1...  5.97 us

profile of v1, /device:TPU:0, one launch (start us, length us, event | category | flops | bytes accessed | tf_op | source)
XLA Modules:
  0.0 96.8 jit_solution(15128212321340166131)
XLA Ops:
  0.6 89.3 %shard_map.67 = (bf16[2048,2048]{1,0:T(8,128)(2,1)S(1)}, bf16[2048,2048]{1,0:T(8,128)(2,1)S(1)}, bf16[32,2048]{1,0:T(8,128)(2,1)}) custom-call(f32[1,512]{1,0:T(1,128)} %bitcast.1, f32[512,2048]{1,0:T(8,128)} %up_w.1, f32[2048,512]{1,0:T(8,128)} %down_w.1, bf16[32,2048]{1,0:T(8,128)(2,1)} %prompt.1), custom_call_target="tpu_custom_call" | custom-call | tf_op jit(solution)/shard_map/pallas_call | solution.py:523
  89.9 0.0 copy-start
  89.9 0.9 copy-done
  90.8 6.0 %shard_map.68 = (bf16[2048,2048]{1,0:T(8,128)(2,1)}, bf16[2048,2048]{1,0:T(8,128)(2,1)}, bf16[32,2048]{1,0:T(8,128)(2,1)}) custom-call(bf16[2048,2048]{1,0:T(8,128)(2,1)S(1)} %get-tuple-element.6.up_v, bf16[2048,2048]{1,0:T(8,128)(2,1)S(1)} %get-tuple-element.7.down_v, bf16[32,2048]{1,0:T(8,128)(2,1)S(1)} %copy-done), custom_call_target="tpu_custom_call" | custom-call | bytes 33554432 | tf_op jit(solution)/shard_map/pallas_call | solution.py:567
Async XLA Ops:
  89.9 0.9 copy-start

commit v2 on v1

--- a/solution.py
+++ b/solution.py
@@ -14,12 +14,12 @@
 READS = 4
 LANES = 128
 K_PIECES = 4
-WHOLE_PART = 0.5
+WHOLE_PART = 0.75
 AHEAD = 2
 STAGE = (0.05, 0.45)
 ARRIVAL = ((0.06, 0.52), (0.13, 0.55), (0.18, 0.78), (0.22, 1.02))
-LAG_Y = 0.2
-ROWS = (0.12, 0.6)
+LAG_Y = 0.4
+ROWS = (0.4, 0.9)
 MESH = pl.DeviceIdType.MESH
 
 
@@ -37,8 +37,8 @@
     gain, up_w, down_w, prompt, up_v, down_v, out_v,
     gain_v, prompt_v, up_f, down_f, gain_col,
     ub, nb, nall, proj, hidden, pbuf, rbuf, stage,
-    in_sem, up_send, stage_recv, z_send, up_recv, upf_send, own_send, own_recv,
-    dn_send, dn_recv, dnf_send, sib_send, sib_recv,
+    in_sem, up_send, stage_recv, z_send, up_recv, up_sib, upf_send, own_send, own_recv,
+    dn_send, dn_recv, dn_sib, dnf_send, sib_send, sib_recv,
     n_send, n_recv, r_send, r_recv,
 ):
     y, z, t = lax.axis_index("grp"), lax.axis_index("fs"), lax.axis_index("tp")
@@ -55,7 +55,7 @@
     x_src, c_src = t_src // CORES, lax.rem(t_src, CORES)
     same_x = x == x_src
 
-    up_part = rows // READS
+    up_part = rows // up_steps
     down_part = units // READS
 
     def up_read(i):
@@ -64,13 +64,14 @@
 
     def down_read(i):
         at = pl.ds(i * down_part, down_part)
-        return pltpu.make_async_copy(down_w.at[at, :], down_f.at[at, :], in_sem.at[2 + READS + i])
+        return pltpu.make_async_copy(down_w.at[at, :], down_f.at[at, :], in_sem.at[2 + up_steps + i])
 
     gain_read = pltpu.make_async_copy(gain, gain_v, in_sem.at[0])
     prompt_read = pltpu.make_async_copy(prompt, prompt_v, in_sem.at[1])
     gain_read.start()
+    up_read(0).start()
     prompt_read.start()
-    for i in range(READS):
+    for i in range(1, up_steps):
         up_read(i).start()
     for i in range(READS):
         down_read(i).start()
@@ -85,12 +86,9 @@
 
     gain_read.wait()
     gain_col[...] = jnp.broadcast_to(gain_v[...], (LANES, rows)).T
-    prompt_read.wait()
-    widened = prompt_v[...].astype(jnp.float32)
-    scale = lax.rsqrt(jnp.mean(widened * widened, axis=-1, keepdims=True) + epsilon)
-    nb[...] = (widened * scale).astype(jnp.bfloat16)
     step = min(16, up_part)
-    for n in range(READS):
+
+    def cast_up(n):
         up_read(n).wait()
 
         @pl.loop(0, up_part // step)
@@ -102,6 +100,7 @@
                     piece = up_f[at, j * units + b * LANES : j * units + (b + 1) * LANES]
                     ub[j, at, b * LANES : (b + 1) * LANES] = (factor * piece).astype(jnp.bfloat16)
 
+    cast_up(0)
     pl.semaphore_wait(barrier, len(peers))
 
     def remote(src, dst, ssem, rsem, dev):
@@ -142,16 +141,16 @@
 
     def up_x(j, m, cd, dx):
         dev = (y, z, lax.rem(x + dx, chips) * CORES + c)
-        sem = up_send.at[j, m, cd, dx]
-        return remote(src_at(j, m, cd), stage.at[x, j, m, cd], sem, stage_recv.at[x, j, m, cd], dev)
+        sems = up_send.at[j, dx - 1], stage_recv.at[dx - 1, j, m]
+        return remote(src_at(j, m, cd), stage.at[dx - 1, j, m, cd], *sems, dev)
 
     def up_x_own(j, m, cd, dx):
         dev = (y, z, lax.rem(x + dx, chips) * CORES + cd)
         k = up_index(m, cd, y)
-        return remote(src_at(j, m, cd), up_at(z, k), up_send.at[j, m, cd, dx], up_recv.at[z, k], dev)
-
-    def up_x_all(act):
-        for m in range(up_steps):
+        return remote(src_at(j, m, cd), up_at(z, k), up_send.at[j, dx - 1], up_recv.at[z, m, y], dev)
+
+    def up_x_all(act, steps):
+        for m in steps:
             for cd in range(CORES):
                 for j in range(ratio):
                     mine = t * ratio + j == z
@@ -166,35 +165,38 @@
 
     def up_z(j, m, cd, dx):
         xs = lax.rem(x + dx, chips)
-        src = src_at(j, m, cd) if dx == 0 else stage.at[xs, j, m, cd]
+        src = src_at(j, m, cd) if dx == 0 else stage.at[chips - dx - 1, j, m, cd]
         k = up_index(m, cd, y)
         dev = (y, (xs * CORES + c) * ratio + j, x * CORES + cd)
-        return remote(src, up_at(z, k), z_send.at[j, m, cd, dx], up_recv.at[z, k], dev)
-
-    def up_z_one(j, m, cd, dx, act):
-        xs = lax.rem(x + dx, chips)
-
-        @pl.when((xs * CORES + c) * ratio + j != z)
-        def _():
-            act(j, m, cd, dx)
-
-    def go_z(j, m, cd, dx):
-        if dx > 0:
-            xs = lax.rem(x + dx, chips)
-            at = stage.at[xs, j, m, cd]
-            remote(at, at, up_send.at[j, m, cd, dx], stage_recv.at[xs, j, m, cd], sibling).wait_recv()
-        up_z(j, m, cd, dx).start()
+        return remote(src, up_at(z, k), z_send.at[j, dx], up_recv.at[z, m, y], dev)
+
+    def away(j, dx, fn):
+        pl.when((lax.rem(x + dx, chips) * CORES + c) * ratio + j != z)(fn)
+
+    def go_z(m, j, dx):
+        def go():
+            if dx > 0:
+                at = stage.at[chips - dx - 1, j, m]
+                remote(at, at, up_send.at[j, 0], stage_recv.at[chips - dx - 1, j, m], sibling).wait_recv()
+            for cd in range(CORES):
+                up_z(j, m, cd, dx).start()
+
+        away(j, dx, go)
 
     def z_own(m):
-        for cd in range(CORES):
-            for j in range(ratio):
-                up_z_one(j, m, cd, 0, go_z)
+        for j in range(ratio):
+            go_z(m, j, 0)
 
     def z_staged(m):
-        for cd in range(CORES):
-            for j in range(ratio):
-                for dx in range(1, chips):
-                    up_z_one(j, m, cd, dx, go_z)
+        for j in range(ratio):
+            for dx in range(1, chips):
+                go_z(m, j, dx)
+
+    def sent(ref, sem):
+        remote(ref, ref, sem, own_recv, sibling).wait_send()
+
+    def landed(ref, sem):
+        remote(ref, ref, own_send, sem, sibling).wait_recv()
 
     own_j = lax.rem(z, ratio)
     own_rows = pl.ds(pl.multiple_of(z * rows, rows), rows)
@@ -212,26 +214,37 @@
     def dn_at(ts, i, k):
         return down_v.at[pl.ds(pl.multiple_of(k * k_rows, k_rows), k_rows), cols_of(ts, i)]
 
-    def dn_first(i, k, dx):
-        dev = (y, z, lax.rem(x + dx, chips) * CORES + c)
-        return remote(dn_at(t, i, k), dn_at(t, i, k), dn_send.at[i, k, dx], dn_recv.at[t, i, k], dev)
-
-    def dn_sends(act):
+    def dn_col(ts, i):
+        return down_v.at[:, cols_of(ts, i)]
+
+    def dn_to(dx):
+        return (y, z, lax.rem(x + dx, chips) * CORES + c)
+
+    def dn_sends():
         for i in range(col_chunks):
-            if i < whole_cols:
-                for k in range(k_pieces):
-                    for dx in range(1, chips):
-                        act(dn_first(i, k, dx))
-            else:
-                for n in range(k_pieces // groups):
-                    for dx in range(1, chips):
-                        act(dn_first(i, n * groups + y, dx))
+            for n in range(1 if i < whole_cols else k_pieces // groups):
+                for dx in range(1, chips):
+                    if i < whole_cols:
+                        at, sem = dn_col(t, i), dn_recv.at[dx - 1, i, 0]
+                    else:
+                        at, sem = dn_at(t, i, n * groups + y), dn_recv.at[dx - 1, i, n * groups + y]
+                    remote(at, at, dn_send.at[int(i < whole_cols), dx - 1], sem, dn_to(dx)).start()
 
     start = lambda copy: copy.start()
-    n_hop(0, start, False)
-    for m in range(min(AHEAD, up_steps)):
-        z_own(m)
-    up_x_all(start)
+    prompt_read.wait()
+    widened = prompt_v[...].astype(jnp.float32)
+    scale = lax.rsqrt(jnp.mean(widened * widened, axis=-1, keepdims=True) + epsilon)
+    nb[...] = (widened * scale).astype(jnp.bfloat16)
+    for m in range(up_steps):
+        if m + 1 < up_steps and m > 0:
+            cast_up(m + 1)
+        up_x_all(start, (m,))
+        if m < AHEAD:
+            z_own(m)
+        if m == 0:
+            n_hop(0, start, False)
+            if up_steps > 1:
+                cast_up(1)
 
     @pl.when(t == t_src)
     def _():
@@ -246,7 +259,7 @@
             at = pl.ds(pl.multiple_of(n * down_part + i * down_step, down_step), down_step)
             down_v[at, my_cols] = down_f[at, :].astype(jnp.bfloat16)
 
-    dn_sends(start)
+    dn_sends()
     sib_copy().start()
 
     n_at(z)[...] = nb[...]
@@ -258,19 +271,17 @@
             part = pl.ds(pl.multiple_of(i * chunk, chunk), chunk)
             up_v[pl.ds(pl.multiple_of(z * rows + i * chunk, chunk), chunk), :] = ub[own_j, part, :]
 
-    def up_y(zr, k, g):
+    def up_y(zr, m, g):
         dev = (lax.rem(y + g, groups), z, t)
-        return remote(up_at(zr, k), up_at(zr, k), upf_send.at[zr, k, g], up_recv.at[zr, k], dev)
-
-    def up_s(zr, k):
-        return remote(up_at(zr, k), up_at(zr, k), upf_send.at[zr, k, 0], up_recv.at[zr, k], sibling)
-
-    def dn_y(ts, i, k, g):
-        dev = (lax.rem(y + g, groups), z, t)
-        return remote(dn_at(ts, i, k), dn_at(ts, i, k), dnf_send.at[ts, i, k, g], dn_recv.at[ts, i, k], dev)
-
-    def dn_s(ts, i, k):
-        return remote(dn_at(ts, i, k), dn_at(ts, i, k), dnf_send.at[ts, i, k, 0], dn_recv.at[ts, i, k], sibling)
+        at = up_at(zr, up_index(m, c, y))
+        return remote(at, at, upf_send.at[zr, g], up_recv.at[zr, m, y], dev)
+
+    def up_s(zr, m, owner):
+        at = up_at(zr, up_index(m, c, owner))
+        return remote(at, at, upf_send.at[zr, 0], up_sib.at[zr], sibling)
+
+    def up_in(zr, m, owner):
+        landed(up_at(zr, up_index(m, c, owner)), up_recv.at[zr, m, owner])
 
     def if_remote(d, fn):
         if d == 0:
@@ -289,11 +300,11 @@
 
     def up_a(m, d):
         def go():
-            zr, k = source(d), up_index(m, c, y)
-            up_s(zr, k).wait_recv()
+            zr = source(d)
+            up_in(zr, m, y)
             for g in range(1, groups):
-                up_y(zr, k, g).start()
-            up_s(zr, k).start()
+                up_y(zr, m, g).start()
+            up_s(zr, m, y).start()
 
         if_remote(d, go)
 
@@ -301,50 +312,46 @@
         def go():
             zr = source(d)
             for g in range(1, groups):
-                k = up_index(m, c, lax.rem(y + g, groups))
-                up_s(zr, k).wait_recv()
-                up_s(zr, k).start()
+                owner = lax.rem(y + g, groups)
+                up_in(zr, m, owner)
+                up_s(zr, m, owner).start()
 
         if_remote(d, go)
 
     def up_c(d):
-        def go():
-            zr = source(d)
-            for m in range(up_steps):
-                for owner in range(groups):
-                    up_s(zr, up_index(m, 1 - c, owner)).wait_recv()
-
-        if_remote(d, go)
+        if_remote(d, lambda: landed(up_v.at[pl.ds(0, rows // CORES), :], up_sib.at[source(d)]))
 
     def up_f(d):
         def go():
             zr = source(d)
-            for m in range(up_steps):
-                for owner in range(groups):
-                    up_s(zr, up_index(m, c, owner)).wait_send()
-                for g in range(1, groups):
-                    up_y(zr, up_index(m, c, y), g).wait_send()
+            sent(up_v.at[pl.ds(0, rows // CORES), :], upf_send.at[zr, 0])
+            for g in range(1, groups):
+                sent(up_v.at[pl.ds(0, rows // (CORES * groups)), :], upf_send.at[zr, g])
 
         if_remote(d, go)
 
     def dn_src(dx):
         return lax.rem(x + dx, chips) * CORES + c
 
-    def dn_one(i, k, dx):
-        ts = dn_src(dx)
-        dn_s(ts, i, k).wait_recv()
-        dn_s(ts, i, k).start()
+    def dn_whole(i, dx):
+        at = dn_col(dn_src(dx), i)
+        landed(at, dn_recv.at[chips - dx - 1, i, 0])
+        remote(at, at, dnf_send.at[dx - 1, 0], dn_sib.at[dx - 1, i], sibling).start()
+
+    def dn_piece(i, k, dx, forward):
+        at, sem = dn_at(dn_src(dx), i, k), dn_recv.at[chips - dx - 1, i, k]
+        landed(at, sem)
+        if forward:
+            for g in range(1, groups):
+                remote(at, at, dnf_send.at[dx - 1, g], sem, (lax.rem(y + g, groups), z, t)).start()
+        remote(at, at, dnf_send.at[dx - 1, 0], dn_sib.at[dx - 1, i], sibling).start()
 
     def dn_a(i, n, dx):
-        ts, k = dn_src(dx), n * groups + y
-        dn_s(ts, i, k).wait_recv()
-        for g in range(1, groups):
-            dn_y(ts, i, k, g).start()
-        dn_s(ts, i, k).start()
+        dn_piece(i, n * groups + y, dx, True)
 
     def dn_b(i, n, dx):
         for g in range(1, groups):
-            dn_one(i, n * groups + lax.rem(y + g, groups), dx)
+            dn_piece(i, n * groups + lax.rem(y + g, groups), dx, False)
 
     part = functools.partial
     events = []
@@ -364,8 +371,7 @@
         events.append((when, part(n_hop, h, start, True)))
     for i in range(whole_cols):
         for dx in range(1, chips):
-            for k in range(k_pieces):
-                events.append((1.1, part(dn_one, i, k, dx)))
+            events.append((1.1, part(dn_whole, i, dx)))
     for _, event in sorted(events, key=lambda e: e[0]):
         event()
 
@@ -407,14 +413,7 @@
     def r_copy(ts, i, wide, d):
         zt = lax.rem(z + d, fs_count)
         cols = pl.ds(pl.multiple_of(ts * width + i * LANES, LANES), wide)
-        sems = r_send.at[ts, i, d], r_recv.at[z, ts, i]
-        return remote(pbuf.at[zt, :, cols], rbuf.at[z, :, cols], *sems, (y, zt, t))
-
-    def r_done(ts, i, wide, d):
-        zr = lax.rem(z + d, fs_count)
-        cols = pl.ds(pl.multiple_of(ts * width + i * LANES, LANES), wide)
-        sems = r_send.at[ts, i, d], r_recv.at[zr, ts, i]
-        remote(pbuf.at[zr, :, cols], rbuf.at[zr, :, cols], *sems, (y, zr, t)).wait()
+        return remote(pbuf.at[zt, :, cols], rbuf.at[z, :, cols], r_send.at[d], r_recv.at[z], (y, zt, t))
 
     def block(ts, i, wide):
         cols = pl.ds(pl.multiple_of(ts * width + i * LANES, LANES), wide)
@@ -440,8 +439,7 @@
                 for n in range(k_pieces // groups):
                     dn_b(i, n, dx)
             if (index - CORES) % CORES == 1:
-                for k in range(k_pieces):
-                    dn_s(ts, i, k).wait_recv()
+                landed(dn_col(ts, i), dn_sib.at[dx - 1, i])
         block(ts, i, wide)
         if index < CORES:
             upto = len(rest) if index == CORES - 1 else (done + len(rest)) // 2
@@ -453,24 +451,34 @@
         last = (ts, i, wide)
     send_block(*last)
 
+    total = pbuf[z].astype(jnp.float32)
+
+    @pl.loop(1, fs_count)
+    def _(d):
+        zr = lax.rem(z + d, fs_count)
+        remote(pbuf.at[zr], rbuf.at[zr], r_send.at[d], r_recv.at[zr], (y, zr, t)).wait()
+
+    for d in range(1, fs_count):
+        total += rbuf[lax.rem(z + d, fs_count)].astype(jnp.float32)
+    out_v[...] = total.astype(jnp.bfloat16)
+
     for d in range(fs_count):
         up_f(d)
     for dx in range(1, chips):
-        ts = dn_src(dx)
-        for i in range(col_chunks):
-            for k in range(k_pieces):
-                dn_s(ts, i, k).wait_send()
-            if i >= whole_cols:
-                for n in range(k_pieces // groups):
-                    for g in range(1, groups):
-                        dn_y(ts, i, n * groups + y, g).wait_send()
-    up_x_all(lambda copy: copy.wait_send())
-    for m in range(up_steps):
-        for cd in range(CORES):
-            for j in range(ratio):
-                for dx in range(chips):
-                    up_z_one(j, m, cd, dx, lambda *at: up_z(*at).wait_send())
-    dn_sends(lambda copy: copy.wait_send())
+        sent(down_v.at[:, pl.ds(0, width)], dnf_send.at[dx - 1, 0])
+        if whole_cols > 0:
+            sent(down_v.at[:, pl.ds(0, whole_cols * LANES)], dn_send.at[1, dx - 1])
+        if whole_cols < col_chunks:
+            half = down_v.at[pl.ds(0, units // groups), pl.ds(0, (col_chunks - whole_cols) * LANES)]
+            sent(half, dn_send.at[0, dx - 1])
+            for g in range(1, groups):
+                sent(half, dnf_send.at[dx - 1, g])
+    for j in range(ratio):
+        half = up_v.at[pl.ds(0, rows // groups), :]
+        for dx in range(1, chips):
+            sent(half, up_send.at[j, dx - 1])
+        for dx in range(chips):
+            away(j, dx, functools.partial(sent, half, z_send.at[j, dx]))
     sib_copy().wait_send()
 
     @pl.when(t == t_src)
@@ -479,16 +487,6 @@
 
     for h in range(fs_count):
         n_hop(h, lambda copy: copy.wait_send(), False)
-
-    total = pbuf[z].astype(jnp.float32)
-    for ts, i, wide in blocks:
-        @pl.loop(1, fs_count)
-        def _(d):
-            r_done(ts, i, wide, d)
-
-    for d in range(1, fs_count):
-        total += rbuf[lax.rem(z + d, fs_count)].astype(jnp.float32)
-    out_v[...] = total.astype(jnp.bfloat16)
 
 
 def write_out(up_v, down_v, out_v, up_out, down_out, mlp_out, sems):
@@ -525,7 +523,7 @@
         out_shape=(
             pltpu.VMEM((depth, units), bf16),
             pltpu.VMEM((units, depth), bf16),
-            jax.ShapeDtypeStruct((tokens, depth), bf16),
+            pltpu.VMEM((tokens, depth), bf16),
         ),
         in_specs=[hbm] * 4,
         out_specs=(vmem,) * 3,
@@ -542,22 +540,24 @@
             pltpu.VMEM((fs_count * tokens, units), bf16),
             pltpu.VMEM((fs_count, tokens, depth), bf16),
             pltpu.VMEM((fs_count, tokens, depth), bf16),
-            pltpu.VMEM((chips, ratio, up_steps, CORES, rows // kc, units), bf16),
-            dma((2 + 2 * READS,)),
-            dma((ratio, up_steps, CORES, chips)),
-            dma((chips, ratio, up_steps, CORES)),
-            dma((ratio, up_steps, CORES, chips)),
-            dma((fs_count, kc)),
-            dma((fs_count, kc, groups)),
+            pltpu.VMEM((chips - 1, ratio, up_steps, CORES, rows // kc, units), bf16),
+            dma((2 + up_steps + READS,)),
+            dma((ratio, chips - 1)),
+            dma((chips - 1, ratio, up_steps)),
+            dma((ratio, chips)),
+            dma((fs_count, up_steps, groups)),
+            dma((fs_count,)),
+            dma((fs_count, groups)),
             dma, dma,
-            dma((col_chunks, k_pieces, chips)),
-            dma((tp_count, col_chunks, k_pieces)),
-            dma((tp_count, col_chunks, k_pieces, groups)),
+            dma((2, chips - 1)),
+            dma((chips - 1, col_chunks, k_pieces)),
+            dma((chips - 1, col_chunks)),
+            dma((chips - 1, groups)),
             dma, dma,
             dma((fs_count, 2)),
             dma((fs_count,)),
-            dma((tp_count, col_chunks, fs_count)),
-            dma((fs_count, tp_count, col_chunks)),
+            dma((fs_count,)),
+            dma((fs_count,)),
         ],
         compiler_params=pltpu.CompilerParams(
             collective_id=0, has_side_effects=True, vmem_limit_bytes=40 * 1024 * 1024

time: 97 us -> 89.9 us (0.927)
  Pallas kernels: 95.3 us -> 89.1 us
    pallas_call x1, Pallas kernels: 89.3 us -> 83.1 us  [per_device(): pl.pallas_call(functools.partial(kernel, groups, fs_count, tp_count, up_s...]
where the time goes in v2:
time: 89.9 us; the launch traced here: 89.7 us
  Pallas kernels  89.1 us (99%)
    pallas_call x1, Pallas kernels, per_device(): pl.pallas_call(functools.partial(kernel, groups, fs_count, tp_count, up_s...  83.1 us
    pallas_call x1, Pallas kernels, per_device(): pl.pallas_call(write_out, out_shape=(jax.ShapeDtypeStruct(up_v.shape, bf1...  5.98 us

profile of v2, /device:TPU:0, one launch (start us, length us, event | category | flops | bytes accessed | tf_op | source)
XLA Modules:
  0.0 89.7 jit_solution(1018213293363624157)
XLA Ops:
  0.6 83.1 %shard_map.67 = (bf16[2048,2048]{1,0:T(8,128)(2,1)S(1)}, bf16[2048,2048]{1,0:T(8,128)(2,1)S(1)}, bf16[32,2048]{1,0:T(8,128)(2,1)S(1)}) custom-call(f32[1,512]{1,0:T(1,128)} %bitcast.1, f32[512,2048]{1,0:T(8,128)} %up_w.1, f32[2048,512]{1,0:T(8,128)} %down_w.1, bf16[32,2048]{1,0:T(8,128)(2,1)} %prompt.1), custom_call_target="tpu_custom_call" | custom-call | tf_op jit(solution)/shard_map/pallas_call | solution.py:521
  83.7 6.0 %shard_map.68 = (bf16[2048,2048]{1,0:T(8,128)(2,1)}, bf16[2048,2048]{1,0:T(8,128)(2,1)}, bf16[32,2048]{1,0:T(8,128)(2,1)}) custom-call(bf16[2048,2048]{1,0:T(8,128)(2,1)S(1)} %get-tuple-element.6.up_v, bf16[2048,2048]{1,0:T(8,128)(2,1)S(1)} %get-tuple-element.7.down_v, bf16[32,2048]{1,0:T(8,128)(2,1)S(1)} %get-tuple-element.8.out_v), custom_call_target="tpu_custom_call" | custom-call | bytes 33554432 | tf_op jit(solution)/shard_map/pallas_call | solution.py:567

commit v3 on v2

--- a/solution.py
+++ b/solution.py
@@ -16,10 +16,13 @@
 K_PIECES = 4
 WHOLE_PART = 0.75
 AHEAD = 2
+FEED = 0.012
+DOWN_TURN = 1.03
+DOWN_CAST = 0.13
 STAGE = (0.05, 0.45)
 ARRIVAL = ((0.06, 0.52), (0.13, 0.55), (0.18, 0.78), (0.22, 1.02))
 LAG_Y = 0.4
-ROWS = (0.4, 0.9)
+ROWS = (0.55, 1.0)
 MESH = pl.DeviceIdType.MESH
 
 
@@ -49,6 +52,12 @@
     width = down_w.shape[1]
     col_chunks = width // LANES
     k_rows = units // k_pieces
+    lead = whole_cols - whole_cols // 2 if col_chunks < 3 else max(0, whole_cols - 1)
+    split = range(lead, lead + col_chunks - whole_cols)
+
+    def whole(i):
+        return i not in split
+
     tokens = prompt.shape[0]
     sibling = (y, z, x * CORES + 1 - c)
     t_src = z // ratio
@@ -222,36 +231,35 @@
 
     def dn_sends():
         for i in range(col_chunks):
-            for n in range(1 if i < whole_cols else k_pieces // groups):
+            for n in range(1 if whole(i) else k_pieces // groups):
                 for dx in range(1, chips):
-                    if i < whole_cols:
+                    if whole(i):
                         at, sem = dn_col(t, i), dn_recv.at[dx - 1, i, 0]
                     else:
                         at, sem = dn_at(t, i, n * groups + y), dn_recv.at[dx - 1, i, n * groups + y]
-                    remote(at, at, dn_send.at[int(i < whole_cols), dx - 1], sem, dn_to(dx)).start()
+                    remote(at, at, dn_send.at[int(whole(i)), dx - 1], sem, dn_to(dx)).start()
 
     start = lambda copy: copy.start()
     prompt_read.wait()
     widened = prompt_v[...].astype(jnp.float32)
     scale = lax.rsqrt(jnp.mean(widened * widened, axis=-1, keepdims=True) + epsilon)
     nb[...] = (widened * scale).astype(jnp.bfloat16)
-    for m in range(up_steps):
-        if m + 1 < up_steps and m > 0:
+    def feed(m):
+        if m + 1 < up_steps:
             cast_up(m + 1)
         up_x_all(start, (m,))
         if m < AHEAD:
             z_own(m)
-        if m == 0:
-            n_hop(0, start, False)
-            if up_steps > 1:
-                cast_up(1)
-
-    @pl.when(t == t_src)
-    def _():
-        own_copy().start()
+
+    up_x_all(start, (0,))
+    z_own(0)
+    n_hop(0, start, False)
+    if up_steps > 1:
+        cast_up(1)
 
     down_step = min(64, down_part)
-    for n in range(READS):
+
+    def cast_down(n):
         down_read(n).wait()
 
         @pl.loop(0, down_part // down_step)
@@ -259,17 +267,21 @@
             at = pl.ds(pl.multiple_of(n * down_part + i * down_step, down_step), down_step)
             down_v[at, my_cols] = down_f[at, :].astype(jnp.bfloat16)
 
-    dn_sends()
-    sib_copy().start()
-
-    n_at(z)[...] = nb[...]
-
-    @pl.when(t == t_src)
-    def _():
-        @pl.loop(0, rows // chunk)
-        def _(i):
-            part = pl.ds(pl.multiple_of(i * chunk, chunk), chunk)
-            up_v[pl.ds(pl.multiple_of(z * rows + i * chunk, chunk), chunk), :] = ub[own_j, part, :]
+    def start_down():
+        dn_sends()
+        sib_copy().start()
+
+    def keep_own():
+        n_at(z)[...] = nb[...]
+
+        @pl.when(t == t_src)
+        def _():
+            own_copy().start()
+
+            @pl.loop(0, rows // chunk)
+            def _(i):
+                part = pl.ds(pl.multiple_of(i * chunk, chunk), chunk)
+                up_v[pl.ds(pl.multiple_of(z * rows + i * chunk, chunk), chunk), :] = ub[own_j, part, :]
 
     def up_y(zr, m, g):
         dev = (lax.rem(y + g, groups), z, t)
@@ -321,7 +333,7 @@
     def up_c(d):
         if_remote(d, lambda: landed(up_v.at[pl.ds(0, rows // CORES), :], up_sib.at[source(d)]))
 
-    def up_f(d):
+    def up_done(d):
         def go():
             zr = source(d)
             sent(up_v.at[pl.ds(0, rows // CORES), :], upf_send.at[zr, 0])
@@ -354,7 +366,13 @@
             dn_piece(i, n * groups + lax.rem(y + g, groups), dx, False)
 
     part = functools.partial
-    events = []
+    events, queued = [], []
+    for m in range(1, up_steps):
+        events.append((FEED * m, part(feed, m)))
+    for n in range(READS):
+        events.append((DOWN_CAST + 0.03 * n, part(cast_down, n)))
+    events.append((DOWN_CAST + 0.03 * READS, start_down))
+    events.append((DOWN_CAST + 0.03 * READS + 0.05, keep_own))
     for m in range(up_steps):
         share = m / max(1, up_steps - 1)
         when = STAGE[0] + (STAGE[1] - STAGE[0]) * share
@@ -369,9 +387,13 @@
     for h in range(1, fs_count):
         when = ROWS[h - 1] if h <= len(ROWS) else 1.2 + h
         events.append((when, part(n_hop, h, start, True)))
-    for i in range(whole_cols):
+    for i in range(lead):
         for dx in range(1, chips):
             events.append((1.1, part(dn_whole, i, dx)))
+    for i in split:
+        for n in range(k_pieces // groups):
+            for dx in range(1, chips):
+                events.append((DOWN_TURN + 0.001 * i, part(dn_a, i, n, dx)))
     for _, event in sorted(events, key=lambda e: e[0]):
         event()
 
@@ -386,10 +408,7 @@
     kb = 256
     nb_tile = min(units, 1024)
 
-    split = range(whole_cols, col_chunks)
-    rest = [part(dn_a, i, n, dx) for i in split for n in range(k_pieces // groups) for dx in range(1, chips)]
     pieces = depth // kb
-    done = 0
     for i in range(pieces):
         for j in range(units // nb_tile):
             col = pl.ds(j * nb_tile, nb_tile)
@@ -402,10 +421,6 @@
                 proj[:, col] = term
             else:
                 proj[:, col] += term
-        upto = len(rest) * (i + 1) // (2 * pieces)
-        for fn in rest[done:upto]:
-            fn()
-        done = upto
 
     positive = jnp.maximum(proj[...], 0.0)
     hidden[...] = (positive * positive).astype(jnp.bfloat16)
@@ -435,17 +450,14 @@
             sib_copy().wait_recv()
         if index >= CORES:
             dx = 1 + (index - CORES) // CORES % (chips - 1)
-            if (index - CORES) % CORES == 0 and i >= whole_cols:
+            if (index - CORES) % CORES == 0 and whole(i) and i >= lead:
+                dn_whole(i, dx)
+            if (index - CORES) % CORES == 0 and not whole(i):
                 for n in range(k_pieces // groups):
                     dn_b(i, n, dx)
             if (index - CORES) % CORES == 1:
                 landed(dn_col(ts, i), dn_sib.at[dx - 1, i])
         block(ts, i, wide)
-        if index < CORES:
-            upto = len(rest) if index == CORES - 1 else (done + len(rest)) // 2
-            for fn in rest[done:upto]:
-                fn()
-            done = upto
         if last is not None:
             send_block(*last)
         last = (ts, i, wide)
@@ -463,7 +475,7 @@
     out_v[...] = total.astype(jnp.bfloat16)
 
     for d in range(fs_count):
-        up_f(d)
+        up_done(d)
     for dx in range(1, chips):
         sent(down_v.at[:, pl.ds(0, width)], dnf_send.at[dx - 1, 0])
         if whole_cols > 0:

time: 89.9 us -> 86.5 us (0.962)
  Pallas kernels: 89.1 us -> 85.7 us
    pallas_call x1, Pallas kernels: 83.1 us -> 79.8 us  [per_device(): pl.pallas_call(functools.partial(kernel, groups, fs_count, tp_count, up_s...]
where the time goes in v3:
time: 86.5 us; the launch traced here: 86.4 us
  Pallas kernels  85.7 us (99%)
    pallas_call x1, Pallas kernels, per_device(): pl.pallas_call(functools.partial(kernel, groups, fs_count, tp_count, up_s...  79.8 us
    pallas_call x1, Pallas kernels, per_device(): pl.pallas_call(write_out, out_shape=(jax.ShapeDtypeStruct(up_v.shape, bf1...  5.98 us

profile of v3, /device:TPU:0, one launch (start us, length us, event | category | flops | bytes accessed | tf_op | source)
XLA Modules:
  0.0 86.4 jit_solution(6710637345544979782)
XLA Ops:
  0.6 79.8 %shard_map.67 = (bf16[2048,2048]{1,0:T(8,128)(2,1)S(1)}, bf16[2048,2048]{1,0:T(8,128)(2,1)S(1)}, bf16[32,2048]{1,0:T(8,128)(2,1)S(1)}) custom-call(f32[1,512]{1,0:T(1,128)} %bitcast.1, f32[512,2048]{1,0:T(8,128)} %up_w.1, f32[2048,512]{1,0:T(8,128)} %down_w.1, bf16[32,2048]{1,0:T(8,128)(2,1)} %prompt.1), custom_call_target="tpu_custom_call" | custom-call | tf_op jit(solution)/shard_map/pallas_call | solution.py:533
  80.4 6.0 %shard_map.68 = (bf16[2048,2048]{1,0:T(8,128)(2,1)}, bf16[2048,2048]{1,0:T(8,128)(2,1)}, bf16[32,2048]{1,0:T(8,128)(2,1)}) custom-call(bf16[2048,2048]{1,0:T(8,128)(2,1)S(1)} %get-tuple-element.6.up_v, bf16[2048,2048]{1,0:T(8,128)(2,1)S(1)} %get-tuple-element.7.down_v, bf16[32,2048]{1,0:T(8,128)(2,1)S(1)} %get-tuple-element.8.out_v), custom_call_target="tpu_custom_call" | custom-call | bytes 33554432 | tf_op jit(solution)/shard_map/pallas_call | solution.py:579

commit v4 on v3

--- a/solution.py
+++ b/solution.py
@@ -22,7 +22,7 @@
 STAGE = (0.05, 0.45)
 ARRIVAL = ((0.06, 0.52), (0.13, 0.55), (0.18, 0.78), (0.22, 1.02))
 LAG_Y = 0.4
-ROWS = (0.55, 1.0)
+ROWS = (0.75, 1.03)
 MESH = pl.DeviceIdType.MESH
 
 

time: 86.5 us -> 85.9 us (level)
  no operation moved by 1% of the time
where the time goes in v4:
time: 85.9 us; the launch traced here: 85.7 us
  Pallas kernels  85.1 us (99%)
    pallas_call x1, Pallas kernels, per_device(): pl.pallas_call(functools.partial(kernel, groups, fs_count, tp_count, up_s...  79.1 us
    pallas_call x1, Pallas kernels, per_device(): pl.pallas_call(write_out, out_shape=(jax.ShapeDtypeStruct(up_v.shape, bf1...  5.98 us

profile of v4, /device:TPU:0, one launch (start us, length us, event | category | flops | bytes accessed | tf_op | source)
XLA Modules:
  0.0 85.7 jit_solution(1665686219879812479)
XLA Ops:
  0.6 79.1 %shard_map.67 = (bf16[2048,2048]{1,0:T(8,128)(2,1)S(1)}, bf16[2048,2048]{1,0:T(8,128)(2,1)S(1)}, bf16[32,2048]{1,0:T(8,128)(2,1)S(1)}) custom-call(f32[1,512]{1,0:T(1,128)} %bitcast.1, f32[512,2048]{1,0:T(8,128)} %up_w.1, f32[2048,512]{1,0:T(8,128)} %down_w.1, bf16[32,2048]{1,0:T(8,128)(2,1)} %prompt.1), custom_call_target="tpu_custom_call" | custom-call | tf_op jit(solution)/shard_map/pallas_call | solution.py:533
  79.7 6.0 %shard_map.68 = (bf16[2048,2048]{1,0:T(8,128)(2,1)}, bf16[2048,2048]{1,0:T(8,128)(2,1)}, bf16[32,2048]{1,0:T(8,128)(2,1)}) custom-call(bf16[2048,2048]{1,0:T(8,128)(2,1)S(1)} %get-tuple-element.6.up_v, bf16[2048,2048]{1,0:T(8,128)(2,1)S(1)} %get-tuple-element.7.down_v, bf16[32,2048]{1,0:T(8,128)(2,1)S(1)} %get-tuple-element.8.out_v), custom_call_target="tpu_custom_call" | custom-call | bytes 33554432 | tf_op jit(solution)/shard_map/pallas_call | solution.py:579
